TPU v7x, 32 devices: a whole 2x2x4 slice. The times are simulated.
32 devices in a mesh: st: 16 (over z, y, x), tp: 2 (over core).
Axes of the slice: x: 2, y: 2, z: 4, core: 2. Of those that a mesh axis runs over, the one named last changes fastest.
Arguments:
- tokens: bfloat16 [12288, 2048], P('st'), may hold values from -6 to 6, as said below
- route_ids: int32 [192, 4], P('st'), may hold values from 0 to 383, as said below
- store: bfloat16 [384, 128, 2048], P('st'), may hold values from -6 to 6, as said below
- token_gain: float32 [2048], replicated, may hold values from 0.1 to 1.9
- store_gain: float32 [2048], replicated, may hold values from 0.1 to 1.9
- carry_weight: bfloat16 [2048, 512], P(None, 'tp'), may hold values from -0.125 to 0.125
- spatial_weight: bfloat16 [2048, 512], P(None, 'tp'), may hold values from -0.125 to 0.125
- spatial_gain: float32 [512], P('tp'), may hold values from 0.1 to 1.9
- position_mix: bfloat16 [8, 128, 128], P('tp'), may hold values from -0.5 to 0.5
- position_bias: float32 [8, 128], P('tp'), may hold values from 0.1 to 1.9
- query_weight: bfloat16 [2048, 512], P(None, 'tp'), may hold values from -0.86178639 to 0.86178639, as said below
- key_weight: bfloat16 [2048, 512], P(None, 'tp'), may hold values from -0.86178639 to 0.86178639, as said below
- read_weight: bfloat16 [2048, 512], P(None, 'tp'), may hold values from -0.125 to 0.125
- blend_weight: bfloat16 [2048, 512], P(None, 'tp'), may hold values from -0.125 to 0.125
- output_weight: bfloat16 [512, 2048], replicated, may hold values from -0.25 to 0.25
Outputs:
- mixed: bfloat16 [12288, 2048], P(('st', 'tp'))
Inputs may be any that keep to these rules, and one draw needn't show every extreme that they name: `route_ids`: each entry is a passage index; passage p is held by index p // 24 of st. All entries of the spans of one index of st (aligned blocks of 12 rows) are different; they name at most 6 passage held by any one index of st, exactly 6 held by the index before their own (cyclically), and at least one held by the index half the axis away. `tokens`: Activations; in some draws the first token of some spans equals a row of a passage that the span reads. `store`: passage rows. `query_weight`: A projection matrix. `key_weight`: A projection matrix.
All inputs are finite; a program needn't handle non-finite values.
Results may differ from a plain program's by a relative error of at most 0.012.
The roundings to bfloat16 on the way count: a program that leaves them out, or rounds other values in their place, can miss the bound.
Values may be sent and summed in bfloat16 or wider, within the bound.
A program may use at most 128 MiB of HBM per device.

v0:
```python
import functools

import jax
import jax.numpy as jnp
from jax import lax
from jax.experimental import pallas as pl
from jax.experimental.pallas import tpu as pltpu
from jax.sharding import PartitionSpec as P

norm_eps = 1e-06
bf16 = jnp.bfloat16
f32 = jnp.float32


def normed_rows(matrix, gain):
    values = matrix.astype(f32)
    scaled = values * lax.rsqrt(jnp.mean(values * values, axis=-1, keepdims=True) + norm_eps)
    return (scaled * gain).astype(bf16)


def query_kernel(span_length, slots, slot_span, tok_ref, gain_ref, wq_ref, normed_ref, sent_ref, q_ref):
    step = pl.program_id(0)
    rows = tok_ref.shape[0]
    normed = normed_rows(tok_ref[...], gain_ref[...])
    normed_ref[...] = normed
    q = jnp.dot(normed, wq_ref[...], preferred_element_type=f32).astype(bf16)
    per = rows // span_length
    for s in range(per):
        q_ref[step * per + s] = q[s * span_length : (s + 1) * span_length]

    @pl.when(step == pl.num_programs(0) - 1)
    def _():
        def body(i, carry):
            sent_ref[i] = q_ref[slot_span[i]]
            return carry

        lax.fori_loop(0, slots, body, 0)


def store_kernel(st_ref, gain_ref, wk_ref, wv_ref, k_ref, vt_ref):
    count, length, _ = st_ref.shape
    for p in range(count):
        normed = normed_rows(st_ref[p], gain_ref[...])
        k_ref[p] = jnp.dot(normed, wk_ref[...], preferred_element_type=f32).astype(bf16)
        v = jnp.dot(normed, wv_ref[...], preferred_element_type=f32)
        vt_ref[p] = v.T.astype(bf16)


def attend(q, k, vt, heads):
    length, width = q.shape
    dim = width // heads
    row_head = lax.broadcasted_iota(jnp.int32, (heads * length, width), 0) // length
    lane_head = lax.broadcasted_iota(jnp.int32, (heads * length, width), 1) // dim
    stacked = jnp.where(row_head == lane_head, jnp.concatenate([q] * heads, axis=0), jnp.zeros((), bf16))
    s = lax.dot_general(k, stacked, (((1,), (1,)), ((), ())), preferred_element_type=f32) * dim ** (-0.5)
    peak = jnp.max(s, axis=0, keepdims=True)
    w = jnp.exp(s - peak)
    total = jnp.sum(w, axis=0, keepdims=True)
    o = jnp.dot(vt, w.astype(bf16), preferred_element_type=f32)
    col_head = lax.broadcasted_iota(jnp.int32, (dim, heads * length), 1) // length
    out = o[0:dim]
    for h in range(1, heads):
        out = jnp.where(col_head == h, o[h * dim : (h + 1) * dim], out)
    return (out / total).astype(bf16), peak + jnp.log(total)


def attention_kernel(heads, ids, q_ref, k_ref, vt_ref, val_ref, lev_ref):
    src = pl.program_id(0)
    cap = q_ref.shape[1]
    for c in range(cap):
        i = ids[src * cap + c]
        val, lev = attend(q_ref[0, c], k_ref[i], vt_ref[i], heads)
        val_ref[0, c] = val
        lev_ref[0, c] = lev


def merge_kernel(heads, spans, picks, pos, val_ref, lev_ref, gated_ref, blend_ref, out_ref):
    step = pl.program_id(0)
    dim, width = val_ref.shape[1:]
    length = width // heads
    for s in range(spans):
        first = (step * spans + s) * picks
        levels = [lev_ref[pos[first + p]] for p in range(picks)]
        top = functools.reduce(jnp.maximum, levels)
        ws = [jnp.exp(lev - top) for lev in levels]
        total = sum(ws)
        summed = sum(w * val_ref[pos[first + p]].astype(f32) for p, w in enumerate(ws))
        mem = (summed / total).T
        mem = jnp.concatenate([mem[h * length : (h + 1) * length] for h in range(heads)], axis=1)
        rows = slice(s * length, (s + 1) * length)
        out_ref[rows] = (gated_ref[rows] + blend_ref[rows] * mem).astype(bf16)


def per_device(
    tokens,
    route_ids,
    store,
    token_gain,
    store_gain,
    carry_weight,
    spatial_weight,
    spatial_gain,
    position_mix,
    position_bias,
    query_weight,
    key_weight,
    read_weight,
    blend_weight,
    output_weight,
):
    row_count, model = tokens.shape
    local_heads, block_length = position_mix.shape[:2]
    width = carry_weight.shape[1]
    head_dim = width // local_heads
    span_count, pick_count = route_ids.shape
    span_length = row_count // span_count
    store_count, passage_length = store.shape[:2]
    owner_count = lax.axis_size("st")
    requests = span_count * pick_count
    cap = max(1, 2 * requests // owner_count)
    slots = owner_count * cap

    flat_ids = route_ids.reshape(requests)
    owner = flat_ids // store_count
    order = jnp.arange(requests, dtype=jnp.int32)
    earlier = (owner[:, None] == owner[None, :]) & (order[None, :] < order[:, None])
    position = owner * cap + jnp.sum(earlier.astype(jnp.int32), axis=1)
    hit = position[None, :] == jnp.arange(slots, dtype=jnp.int32)[:, None]
    slot_local = jnp.sum(jnp.where(hit, (flat_ids % store_count)[None, :], 0), axis=1)
    slot_span = jnp.sum(jnp.where(hit, (order // pick_count)[None, :], 0), axis=1)
    piece_local = lax.all_to_all(
        slot_local.reshape(owner_count, cap), "st", split_axis=0, concat_axis=0, tiled=True
    ).reshape(slots)

    tile = 2 * span_length
    normed, sent = pl.pallas_call(
        functools.partial(query_kernel, span_length, slots),
        grid_spec=pltpu.PrefetchScalarGridSpec(
            num_scalar_prefetch=1,
            grid=(row_count // tile,),
            in_specs=[
                pl.BlockSpec((tile, model), lambda i, _: (i, 0)),
                pl.BlockSpec((1, model), lambda i, _: (0, 0)),
                pl.BlockSpec((model, width), lambda i, _: (0, 0)),
            ],
            out_specs=[
                pl.BlockSpec((tile, model), lambda i, _: (i, 0)),
                pl.BlockSpec((slots, span_length, width), lambda i, _: (0, 0, 0)),
            ],
            scratch_shapes=[pltpu.VMEM((span_count, span_length, width), bf16)],
        ),
        out_shape=[
            jax.ShapeDtypeStruct((row_count, model), bf16),
            jax.ShapeDtypeStruct((slots, span_length, width), bf16),
        ],
        cost_estimate=pl.CostEstimate(
            flops=2 * row_count * model * width, bytes_accessed=4 * row_count * model, transcendentals=0
        ),
        name="query",
    )(slot_span, tokens, token_gain.reshape(1, model), query_weight)
    piece_q = lax.all_to_all(
        sent.reshape(owner_count, cap, span_length, width), "st", split_axis=0, concat_axis=0, tiled=True
    )

    group = 2
    keys, values_t = pl.pallas_call(
        store_kernel,
        grid=(store_count // group,),
        in_specs=[
            pl.BlockSpec((group, passage_length, model), lambda i: (i, 0, 0)),
            pl.BlockSpec((1, model), lambda i: (0, 0)),
            pl.BlockSpec((model, width), lambda i: (0, 0)),
            pl.BlockSpec((model, width), lambda i: (0, 0)),
        ],
        out_specs=[
            pl.BlockSpec((group, passage_length, width), lambda i: (i, 0, 0)),
            pl.BlockSpec((group, width, passage_length), lambda i: (i, 0, 0)),
        ],
        out_shape=[
            jax.ShapeDtypeStruct((store_count, passage_length, width), bf16),
            jax.ShapeDtypeStruct((store_count, width, passage_length), bf16),
        ],
        cost_estimate=pl.CostEstimate(
            flops=4 * store_count * passage_length * model * width,
            bytes_accessed=2 * store_count * passage_length * model,
            transcendentals=0,
        ),
        name="store",
    )(store, store_gain.reshape(1, model), key_weight, read_weight)

    part_values, part_levels = pl.pallas_call(
        functools.partial(attention_kernel, local_heads),
        grid_spec=pltpu.PrefetchScalarGridSpec(
            num_scalar_prefetch=1,
            grid=(owner_count,),
            in_specs=[
                pl.BlockSpec((1, cap, span_length, width), lambda i, _: (i, 0, 0, 0)),
                pl.BlockSpec((store_count, passage_length, width), lambda i, _: (0, 0, 0)),
                pl.BlockSpec((store_count, width, passage_length), lambda i, _: (0, 0, 0)),
            ],
            out_specs=[
                pl.BlockSpec((1, cap, head_dim, local_heads * span_length), lambda i, _: (i, 0, 0, 0)),
                pl.BlockSpec((1, cap, 1, local_heads * span_length), lambda i, _: (i, 0, 0, 0)),
            ],
        ),
        out_shape=[
            jax.ShapeDtypeStruct((owner_count, cap, head_dim, local_heads * span_length), bf16),
            jax.ShapeDtypeStruct((owner_count, cap, 1, local_heads * span_length), f32),
        ],
        name="attention",
    )(piece_local, piece_q, keys, values_t)
    back_values = lax.all_to_all(part_values, "st", split_axis=0, concat_axis=0, tiled=True)
    back_levels = lax.all_to_all(part_levels, "st", split_axis=0, concat_axis=0, tiled=True)

    carry_branch = jnp.dot(normed, carry_weight, preferred_element_type=f32)
    spatial = jax.nn.gelu(jnp.dot(normed, spatial_weight, preferred_element_type=f32), approximate=False)
    total_width = width * lax.axis_size("tp")
    moment_one, moment_two = lax.psum(
        (jnp.sum(spatial, axis=1), jnp.sum(spatial * spatial, axis=1)), "tp"
    )
    channel_mean = (moment_one / total_width)[:, None]
    channel_spread = (moment_two / total_width)[:, None] - channel_mean * channel_mean
    spatial_in = (
        (spatial - channel_mean) * lax.rsqrt(channel_spread + norm_eps) * spatial_gain
    ).astype(bf16)
    blocks = spatial_in.reshape(row_count // block_length, block_length, local_heads, head_dim)
    mixed_blocks = jnp.einsum("hij,njhc->nihc", position_mix, blocks, preferred_element_type=f32)
    mixed_blocks = mixed_blocks + position_bias.T[None, :, :, None]
    gated_mix = jax.nn.gelu(carry_branch, approximate=False) * mixed_blocks.reshape(row_count, width)
    blend_gate = jax.nn.sigmoid(jnp.dot(normed, blend_weight, preferred_element_type=f32))

    spans = 4 if span_count % 4 == 0 else 1
    mixed_rows = pl.pallas_call(
        functools.partial(merge_kernel, local_heads, spans, pick_count),
        grid_spec=pltpu.PrefetchScalarGridSpec(
            num_scalar_prefetch=1,
            grid=(span_count // spans,),
            in_specs=[
                pl.BlockSpec((slots, head_dim, local_heads * span_length), lambda i, _: (0, 0, 0)),
                pl.BlockSpec((slots, 1, local_heads * span_length), lambda i, _: (0, 0, 0)),
                pl.BlockSpec((spans * span_length, width), lambda i, _: (i, 0)),
                pl.BlockSpec((spans * span_length, width), lambda i, _: (i, 0)),
            ],
            out_specs=pl.BlockSpec((spans * span_length, width), lambda i, _: (i, 0)),
        ),
        out_shape=jax.ShapeDtypeStruct((row_count, width), bf16),
        name="merge",
    )(
        position,
        back_values.reshape(slots, head_dim, local_heads * span_length),
        back_levels.reshape(slots, 1, local_heads * span_length),
        gated_mix,
        blend_gate,
    )
    by_rows = lax.all_to_all(mixed_rows, "tp", split_axis=0, concat_axis=1, tiled=True)
    return jnp.dot(by_rows, output_weight, preferred_element_type=f32).astype(bf16)


def solution(mesh):
    in_specs = (
        P("st", None),
        P("st", None),
        P("st", None, None),
        P(),
        P(),
        P(None, "tp"),
        P(None, "tp"),
        P("tp"),
        P("tp", None, None),
        P("tp", None),
        P(None, "tp"),
        P(None, "tp"),
        P(None, "tp"),
        P(None, "tp"),
        P(),
    )
    out_specs = P(("st", "tp"), None)
    return jax.shard_map(
        per_device, mesh=mesh, in_specs=in_specs, out_specs=out_specs, check_vma=False
    )
```

profile of v0, /device:TPU:13, one launch (start us, length us, event | category | flops | bytes accessed | tf_op | source)
XLA Modules:
  0.0 215.4 jit_solution(2568718729833888557)
XLA Ops:
  0.0 0.0 copy-start
  0.0 0.8 sign_compare_fusion
  0.8 0.7 broadcast_remainder_fusion
  1.5 0.1 copy.44
  1.6 0.1 ne.74
  1.7 0.1 copy.45
  1.8 0.1 rem.39
  1.9 0.1 copy.46
  2.0 0.1 div.36
  2.1 0.2 convert_reduce_fusion
  2.3 0.0 copy-start.3
  2.3 0.7 select_reduce_fusion
  3.0 0.7 all_to_all.29
  3.7 6.6 %all-to-all-start = ((s32[16,1,6]{2,1,0:T(1,128)}), s32[16,1,6]{2,1,0:T(1,128)S(1)}, u32[]{:S(2)}, u32[]{:S(2)}) async-start(s32[16,1,6]{2,1,0:T(1,128)} %bitcast), calls=%async_computation | async-start | bytes 16384 | tf_op jit(solution)/shard_map/all_to_all | solution.py:131
  10.3 9.1 %query.1 = (bf16[768,2048]{1,0:T(8,128)(2,1)}, bf16[96,64,256]{2,1,0:T(8,128)(2,1)}) custom-call(s32[96]{0:T(128)} %get-tuple-element.19.slot_span, bf16[768,2048]{1,0:T(8,128)(2,1)} %tok_ref.1, f32[1,2048]{1,0:T(1,128)} %bitcast.32, bf16[2048,256]{1,0:T(8,128)(2,1)} %wq_ref.1), custom_call_target="tpu_custom_call" | custom-call | flops 805306368 | bytes 6291456 | tf_op jit(solution)/shard_map/query/pallas_call | solution.py:136
  19.4 0.0 all-to-all-done
  19.4 0.0 copy-done.3
  19.4 6.4 %all-to-all-start.1 = ((bf16[16,6,64,256]{3,2,1,0:T(8,128)(2,1)}), bf16[16,6,64,256]{3,2,1,0:T(8,128)(2,1)}, u32[]{:S(2)}, u32[]{:S(2)}) async-start(bf16[16,6,64,256]{3,2,1,0:T(8,128)(2,1)} %bitcast.28), calls=%async_computation.1 | async-start | bytes 6291456 | tf_op jit(solution)/shard_map/all_to_all | solution.py:161
  25.8 15.8 %store.1 = (bf16[24,128,256]{2,1,0:T(8,128)(2,1)}, bf16[24,256,128]{2,1,0:T(8,128)(2,1)}) custom-call(bf16[24,128,2048]{2,1,0:T(8,128)(2,1)} %st_ref.1, f32[1,2048]{1,0:T(1,128)} %bitcast.34, bf16[2048,256]{1,0:T(8,128)(2,1)} %wk_ref.1, bf16[2048,256]{1,0:T(8,128)(2,1)} %wv_ref.1), custom_call_target="tpu_custom_call" | custom-call | flops 6442450944 | bytes 12582912 | tf_op jit(solution)/shard_map/store/pallas_call | solution.py:166
  41.6 0.6 broadcast.309
  42.2 0.7 reduce.3
  42.9 0.7 reshape.115.ids
  43.5 52.7 %all-to-all-done.1.q_ref = bf16[16,6,64,256]{3,2,1,0:T(8,128)(2,1)} async-done(((bf16[16,6,64,256]{3,2,1,0:T(8,128)(2,1)}), bf16[16,6,64,256]{3,2,1,0:T(8,128)(2,1)}, u32[]{:S(2)}, u32[]{:S(2)}) %all-to-all-start.1) | async-done | bytes 3145760 | tf_op jit(solution)/shard_map/all_to_all | solution.py:161
  96.2 19.5 %attention.1 = (bf16[16,6,64,256]{3,2,1,0:T(8,128)(2,1)}, f32[16,6,1,256]{3,2,1,0:T(1,128)}) custom-call(s32[96]{0:T(128)} %reshape.115.ids, bf16[16,6,64,256]{3,2,1,0:T(8,128)(2,1)} %all-to-all-done.1.q_ref, bf16[24,128,256]{2,1,0:T(8,128)(2,1)} %get-tuple-element.12.k_ref, bf16[24,256,128]{2,1,0:T(8,128)(2,1)} %get-tuple-element.13.vt_ref), custom_call_target="tpu_custom_call" | custom-call | tf_op jit(solution)/shard_map/attention/pallas_call | solution.py:191
  115.7 9.4 %all_to_all.43 = f32[16,6,1,256]{3,2,1,0:T(1,128)} all-to-all(f32[16,6,1,256]{3,2,1,0:T(1,128)} %get-tuple-element.15), channel_id=1, replica_groups=mesh['st'=16,'tp'=2] {'st'}, dimensions={0} | all-to-all | bytes 196608 | tf_op jit(solution)/shard_map/all_to_all | solution.py:213
  125.0 6.1 %all-to-all-start.2 = ((bf16[16,6,64,256]{3,2,1,0:T(8,128)(2,1)}), bf16[16,6,64,256]{3,2,1,0:T(8,128)(2,1)}, u32[]{:S(2)}, u32[]{:S(2)}) async-start(bf16[16,6,64,256]{3,2,1,0:T(8,128)(2,1)} %get-tuple-element.14), calls=%async_computation.2 | async-start | bytes 6291456 | tf_op jit(solution)/shard_map/all_to_all | solution.py:212
  131.2 0.0 copy-start.1
  131.2 0.0 copy-start.2
  131.2 4.9 %fusion.26 = (f32[768]{0:T(1024)S(1)}, f32[768]{0:T(1024)S(1)}, f32[768,256]{1,0:T(8,128)S(1)}) fusion(bf16[768,2048]{1,0:T(8,128)(2,1)} %get-tuple-element.16, bf16[2048,256]{1,0:T(8,128)(2,1)} %param.21), kind=kOutput, calls=%fused_computation.66 | convolution fusion | flops 818477568 | bytes 4986880 | tf_op jit(solution)/shard_map/dot_general | solution.py:216
  136.0 5.2 %all-reduce = (f32[768]{0:T(1024)S(1)}, f32[768]{0:T(1024)S(1)}) all-reduce(f32[768]{0:T(1024)S(1)} %get-tuple-element.18, f32[768]{0:T(1024)S(1)} %get-tuple-element.17), channel_id=1, replica_groups=mesh['st'=16,'tp'=2] {'tp'}, use_global_device_ids=true, to_apply=%region_6.7 | all-reduce | flops 1536 | bytes 12288 | tf_op jit(solution)/shard_map/psum | solution.py:218
  141.3 0.0 copy-done.4
  141.3 0.3 multiply_convert_fusion
  141.6 0.3 reshape.124
  141.9 0.0 copy-done.1
  141.9 0.0 copy-done.2
  141.9 1.3 fusion.1
  143.2 2.4 %copy.59 = f32[6,128,4,64]{3,2,1,0:T(4,128)} copy(f32[6,128,4,64]{1,3,0,2:T(8,128)} %fusion.1) | data formatting | bytes 1572864 | tf_op jit(solution)/shard_map/reshape | solution.py:229
  145.6 2.2 %reshape.125 = f32[768,256]{1,0:T(8,128)S(1)} reshape(f32[6,128,4,64]{3,2,1,0:T(4,128)} %copy.59) | data formatting | bytes 1572864 | tf_op jit(solution)/shard_map/reshape | solution.py:229
  147.9 0.0 copy-start.5
  147.9 0.0 copy-start.6
  147.9 4.2 %fusion.3.blend_ref = f32[768,256]{1,0:T(8,128)} fusion(bf16[768,2048]{1,0:T(8,128)(2,1)} %get-tuple-element.16, bf16[2048,256]{1,0:T(8,128)(2,1)} %param.28), kind=kOutput, calls=%fused_computation.6 | convolution fusion | flops 805896192 | bytes 4980736 | tf_op jit(solution)/shard_map/dot_general | solution.py:230
  152.1 0.0 copy-done.5
  152.1 3.4 %fusion.6.gated_ref = f32[768,256]{1,0:T(8,128)} fusion(f32[768,256]{1,0:T(8,128)S(1)} %reshape.125, bf16[768,2048]{1,0:T(8,128)(2,1)S(1)} %copy-done.5, bf16[2048,256]{1,0:T(8,128)(2,1)S(1)} %copy-done.6), kind=kOutput, calls=%fused_computation.11 | convolution fusion | flops 818085888 | bytes 5767168 | tf_op jit(solution)/shard_map/dot_general | solution.py:215
  155.5 46.3 %all-to-all-done.2 = bf16[16,6,64,256]{3,2,1,0:T(8,128)(2,1)} async-done(((bf16[16,6,64,256]{3,2,1,0:T(8,128)(2,1)}), bf16[16,6,64,256]{3,2,1,0:T(8,128)(2,1)}, u32[]{:S(2)}, u32[]{:S(2)}) %all-to-all-start.2) | async-done | bytes 3145760 | tf_op jit(solution)/shard_map/all_to_all | solution.py:212
  201.8 5.1 %merge.1 = bf16[768,256]{1,0:T(8,128)(2,1)} custom-call(s32[48]{0:T(128)} %copy-done.3, bf16[96,64,256]{2,1,0:T(8,128)(2,1)} %bitcast.4.val_ref, f32[96,1,256]{2,1,0:T(1,128)} %bitcast.31, f32[768,256]{1,0:T(8,128)} %fusion.6.gated_ref, f32[768,256]{1,0:T(8,128)} %fusion.3.blend_ref), custom_call_target="tpu_custom_call" | custom-call | tf_op jit(solution)/shard_map/merge/pallas_call | solution.py:233
  206.9 1.2 copy.54
  208.2 5.1 %all_to_all.44 = bf16[2,384,256]{1,2,0:T(8,128)(2,1)S(1)} all-to-all(bf16[2,384,256]{1,2,0:T(8,128)(2,1)S(1)} %copy.54), channel_id=1, replica_groups=mesh['st'=16,'tp'=2] {'tp'}, dimensions={0} | all-to-all | bytes 786432 | tf_op jit(solution)/shard_map/all_to_all | solution.py:255
  213.3 2.2 %convolution_convert_fusion = bf16[384,2048]{1,0:T(8,128)(2,1)} fusion(bf16[384,512]{0,1:T(8,128)(2,1)S(1)} %bitcast.30, bf16[512,2048]{1,0:T(8,128)(2,1)S(1)} %copy-done), kind=kOutput, calls=%fused_computation | convolution fusion | flops 806092800 | bytes 4063232 | tf_op jit(solution)/shard_map/dot_general | solution.py:256
  (6 shorter events, 0.0 us)
Async XLA Ops:
  0.0 213.3 %copy-start = (bf16[512,2048]{1,0:T(8,128)(2,1)S(1)}, bf16[512,2048]{1,0:T(8,128)(2,1)}, u32[]{:S(2)}) copy-start(bf16[512,2048]{1,0:T(8,128)(2,1)} %param.29) | copy-start | bytes 6291460
  2.3 17.1 %copy-start.3 = (s32[48]{0:T(128)}, s32[48]{0:T(128)S(1)}, u32[]{:S(2)}) copy-start(s32[48]{0:T(128)S(1)} %multiply_add_fusion.pos) | copy-start | bytes 580
  3.7 15.7 %all-to-all-start = ((s32[16,1,6]{2,1,0:T(1,128)}), s32[16,1,6]{2,1,0:T(1,128)S(1)}, u32[]{:S(2)}, u32[]{:S(2)}) async-start(s32[16,1,6]{2,1,0:T(1,128)} %bitcast), calls=%async_computation | async-start | bytes 16384 | tf_op jit(solution)/shard_map/all_to_all | solution.py:131
  19.4 76.8 %all-to-all-start.1 = ((bf16[16,6,64,256]{3,2,1,0:T(8,128)(2,1)}), bf16[16,6,64,256]{3,2,1,0:T(8,128)(2,1)}, u32[]{:S(2)}, u32[]{:S(2)}) async-start(bf16[16,6,64,256]{3,2,1,0:T(8,128)(2,1)} %bitcast.28), calls=%async_computation.1 | async-start | bytes 6291456 | tf_op jit(solution)/shard_map/all_to_all | solution.py:161
  125.0 76.8 %all-to-all-start.2 = ((bf16[16,6,64,256]{3,2,1,0:T(8,128)(2,1)}), bf16[16,6,64,256]{3,2,1,0:T(8,128)(2,1)}, u32[]{:S(2)}, u32[]{:S(2)}) async-start(bf16[16,6,64,256]{3,2,1,0:T(8,128)(2,1)} %get-tuple-element.14), calls=%async_computation.2 | async-start | bytes 6291456 | tf_op jit(solution)/shard_map/all_to_all | solution.py:212
  131.2 10.1 %copy-start.4 = (f32[256]{0:T(256)S(1)}, f32[256]{0:T(256)}, u32[]{:S(2)}) copy-start(f32[256]{0:T(256)} %param.22) | copy-start | bytes 3076
  131.2 10.7 %copy-start.1 = (bf16[4,128,128]{2,1,0:T(8,128)(2,1)S(1)}, bf16[4,128,128]{2,1,0:T(8,128)(2,1)}, u32[]{:S(2)}) copy-start(bf16[4,128,128]{2,1,0:T(8,128)(2,1)} %param.23) | copy-start | bytes 393220
  131.2 10.7 %copy-start.2 = (f32[4,128]{1,0:T(4,128)S(1)}, f32[4,128]{1,0:T(4,128)}, u32[]{:S(2)}) copy-start(f32[4,128]{1,0:T(4,128)} %param.24) | copy-start | bytes 6148
  147.9 4.2 %copy-start.5 = (bf16[768,2048]{1,0:T(8,128)(2,1)S(1)}, bf16[768,2048]{1,0:T(8,128)(2,1)}, u32[]{:S(2)}) copy-start(bf16[768,2048]{1,0:T(8,128)(2,1)} %get-tuple-element.16) | copy-start | bytes 9437188
  147.9 4.2 %copy-start.6 = (bf16[2048,256]{1,0:T(8,128)(2,1)S(1)}, bf16[2048,256]{1,0:T(8,128)(2,1)}, u32[]{:S(2)}) copy-start(bf16[2048,256]{1,0:T(8,128)(2,1)} %param.20) | copy-start | bytes 3145732
where the time goes:
time: 217 us; the launch traced here: 215 us
  waiting for transfers between devices  99 us (46%)
  Pallas kernels  49.5 us (23%)
  blocking collectives  19.7 us (9%)
  starting transfers between devices  19.1 us (9%)
  matrix products  15.9 us (7%)
  local copies, waits for them, and re-layouts  8.72 us (4%)
  other arithmetic  3.38 us (2%)
    all_to_all x1, waiting for transfers between devices, per_device(): lax.all_to_all(sent.reshape(owner_count, cap, span_length, width), 'st',...  52.7 us
    all_to_all x1, waiting for transfers between devices, per_device(): lax.all_to_all(part_values, 'st', split_axis=0, concat_axis=0, tiled=True)  46.3 us
    pallas_call x1, Pallas kernels, per_device(): pl.pallas_call(functools.partial(attention_kernel, local_heads), grid_spe...  19.5 us
    pallas_call x1, Pallas kernels, per_device(): pl.pallas_call(store_kernel, grid=(store_count // group,), in_specs=[pl.B...  15.8 us
    all_to_all x1, blocking collectives, per_device(): lax.all_to_all(part_levels, 'st', split_axis=0, concat_axis=0, tiled=True)  9.35 us
    pallas_call x1, Pallas kernels, per_device(): pl.pallas_call(functools.partial(query_kernel, span_length, slots), grid_...  9.09 us
    all_to_all x1, starting transfers between devices, per_device(): lax.all_to_all(slot_local.reshape(owner_count, cap), 'st', split_axis=0,...  6.61 us
    all_to_all x1, starting transfers between devices, per_device(): lax.all_to_all(sent.reshape(owner_count, cap, span_length, width), 'st',...  6.37 us
  transfers between devices with their start and end apart: 3, of which 2 were waited for; matrix products, arithmetic and copies ran while one was open for 10% of the time, Pallas kernels for 12%

commit v1 on v0

--- a/solution.py
+++ b/solution.py
@@ -64,14 +64,71 @@
     return (out / total).astype(bf16), peak + jnp.log(total)
 
 
-def attention_kernel(heads, ids, q_ref, k_ref, vt_ref, val_ref, lev_ref):
-    src = pl.program_id(0)
+def attention_kernel(heads, n, ids, q_ref, k_ref, vt_ref, val_ref, lev_ref, out_val, out_lev, send, recv):
+    me = lax.axis_index("st")
     cap = q_ref.shape[1]
-    for c in range(cap):
-        i = ids[src * cap + c]
-        val, lev = attend(q_ref[0, c], k_ref[i], vt_ref[i], heads)
-        val_ref[0, c] = val
-        lev_ref[0, c] = lev
+
+    barrier = pltpu.get_barrier_semaphore()
+
+    def greet(d, carry):
+        pl.semaphore_signal(
+            barrier,
+            inc=1,
+            device_id={"st": lax.rem(me + d, n)},
+            device_id_type=pl.DeviceIdType.MESH,
+        )
+        return carry
+
+    lax.fori_loop(1, n, greet, 0)
+    pl.semaphore_wait(barrier, n - 1)
+
+    def compute(dst, val_to, lev_to):
+        for c in range(cap):
+            i = ids[dst * cap + c]
+            val, lev = attend(q_ref[dst, c], k_ref[i], vt_ref[i], heads)
+            val_to[dst, c] = val
+            lev_to[dst, c : c + 1] = lev
+
+    def copies(d):
+        dst = lax.rem(me + d, n)
+        pairs = ((out_val, val_ref), (out_lev, lev_ref))
+        return [
+            pltpu.make_async_remote_copy(
+                src_ref=src.at[dst],
+                dst_ref=to.at[me],
+                send_sem=send.at[j, d],
+                recv_sem=recv.at[j, d],
+                device_id={"st": dst},
+                device_id_type=pl.DeviceIdType.MESH,
+            )
+            for j, (src, to) in enumerate(pairs)
+        ]
+
+    def offset(i):
+        j = n // 2 + i
+        return j % n + j // n
+
+    def launch(d):
+        for copy in copies(d):
+            copy.start()
+
+    compute(lax.rem(me + offset(0), n), out_val, out_lev)
+
+    def step(i, carry):
+        compute(lax.rem(me + offset(i), n), out_val, out_lev)
+        launch(offset(i - 1))
+        return carry
+
+    lax.fori_loop(1, n - 1, step, 0)
+    compute(me, val_ref, lev_ref)
+    launch(offset(n - 2))
+
+    def finish(d, carry):
+        for copy in copies(d):
+            copy.wait()
+        return carry
+
+    lax.fori_loop(1, n, finish, 0)
 
 
 def merge_kernel(heads, spans, picks, pos, val_ref, lev_ref, gated_ref, blend_ref, out_ref):
@@ -188,30 +245,6 @@
         name="store",
     )(store, store_gain.reshape(1, model), key_weight, read_weight)
 
-    part_values, part_levels = pl.pallas_call(
-        functools.partial(attention_kernel, local_heads),
-        grid_spec=pltpu.PrefetchScalarGridSpec(
-            num_scalar_prefetch=1,
-            grid=(owner_count,),
-            in_specs=[
-                pl.BlockSpec((1, cap, span_length, width), lambda i, _: (i, 0, 0, 0)),
-                pl.BlockSpec((store_count, passage_length, width), lambda i, _: (0, 0, 0)),
-                pl.BlockSpec((store_count, width, passage_length), lambda i, _: (0, 0, 0)),
-            ],
-            out_specs=[
-                pl.BlockSpec((1, cap, head_dim, local_heads * span_length), lambda i, _: (i, 0, 0, 0)),
-                pl.BlockSpec((1, cap, 1, local_heads * span_length), lambda i, _: (i, 0, 0, 0)),
-            ],
-        ),
-        out_shape=[
-            jax.ShapeDtypeStruct((owner_count, cap, head_dim, local_heads * span_length), bf16),
-            jax.ShapeDtypeStruct((owner_count, cap, 1, local_heads * span_length), f32),
-        ],
-        name="attention",
-    )(piece_local, piece_q, keys, values_t)
-    back_values = lax.all_to_all(part_values, "st", split_axis=0, concat_axis=0, tiled=True)
-    back_levels = lax.all_to_all(part_levels, "st", split_axis=0, concat_axis=0, tiled=True)
-
     carry_branch = jnp.dot(normed, carry_weight, preferred_element_type=f32)
     spatial = jax.nn.gelu(jnp.dot(normed, spatial_weight, preferred_element_type=f32), approximate=False)
     total_width = width * lax.axis_size("tp")
@@ -228,6 +261,25 @@
     mixed_blocks = mixed_blocks + position_bias.T[None, :, :, None]
     gated_mix = jax.nn.gelu(carry_branch, approximate=False) * mixed_blocks.reshape(row_count, width)
     blend_gate = jax.nn.sigmoid(jnp.dot(normed, blend_weight, preferred_element_type=f32))
+
+    keys, gated_mix, blend_gate = lax.optimization_barrier((keys, gated_mix, blend_gate))
+    value_shape = (owner_count, cap, head_dim, local_heads * span_length)
+    level_shape = (owner_count, cap, local_heads * span_length)
+    vmem = pl.BlockSpec(memory_space=pltpu.VMEM)
+    back_values, back_levels = pl.pallas_call(
+        functools.partial(attention_kernel, local_heads, owner_count),
+        in_specs=[pl.BlockSpec(memory_space=pltpu.SMEM), vmem, vmem, vmem],
+        out_specs=[vmem, vmem],
+        out_shape=[jax.ShapeDtypeStruct(value_shape, bf16), jax.ShapeDtypeStruct(level_shape, f32)],
+        scratch_shapes=[
+            pltpu.VMEM(value_shape, bf16),
+            pltpu.VMEM(level_shape, f32),
+            pltpu.SemaphoreType.DMA((2, owner_count)),
+            pltpu.SemaphoreType.DMA((2, owner_count)),
+        ],
+        compiler_params=pltpu.CompilerParams(collective_id=0, has_side_effects=True),
+        name="attention",
+    )(piece_local, piece_q, keys, values_t)
 
     spans = 4 if span_count % 4 == 0 else 1
     mixed_rows = pl.pallas_call(

time: 217 us -> 196 us (0.903)
  the two profiles are of different devices: /device:TPU:13 before, /device:TPU:0 now
where the time goes in v1:
time: 196 us; the launch traced here: 195 us
  Pallas kernels  122 us (62%)
  waiting for transfers between devices  19.6 us (10%)
  matrix products  17.9 us (9%)
  starting transfers between devices  15.3 us (8%)
  local copies, waits for them, and re-layouts  10.2 us (5%)
  blocking collectives  6.55 us (3%)
  other arithmetic  3.29 us (2%)
    pallas_call x1, Pallas kernels, per_device(): pl.pallas_call(functools.partial(attention_kernel, local_heads, owner_cou...  92.3 us
    all_to_all x1, waiting for transfers between devices, per_device(): lax.all_to_all(sent.reshape(owner_count, cap, span_length, width), 'st',...  19.6 us
    pallas_call x1, Pallas kernels, per_device(): pl.pallas_call(store_kernel, grid=(store_count // group,), in_specs=[pl.B...  15.8 us
    pallas_call x1, Pallas kernels, per_device(): pl.pallas_call(functools.partial(query_kernel, span_length, slots), grid_...  9.21 us
    all_to_all x1, starting transfers between devices, per_device(): lax.all_to_all(slot_local.reshape(owner_count, cap), 'st', split_axis=0,...  8.34 us
    all_to_all x1, starting transfers between devices, per_device(): lax.all_to_all(sent.reshape(owner_count, cap, span_length, width), 'st',...  6.96 us
    dot_general x1, matrix products, per_device(): carry_branch = jnp.dot(normed, carry_weight, preferred_element_type=f32)  5.56 us
    pallas_call x1, Pallas kernels, per_device(): pl.pallas_call(functools.partial(merge_kernel, local_heads, spans, pick_c...  5.14 us
  transfers between devices with their start and end apart: 2, of which 1 were waited for; matrix products, arithmetic and copies ran while one was open for 12% of the time, Pallas kernels for 13%

profile of v1, /device:TPU:0, one launch (start us, length us, event | category | flops | bytes accessed | tf_op | source)
XLA Modules:
  0.0 195.4 jit_solution(7383409042361852117)
XLA Ops:
  0.0 0.0 copy-start
  0.0 0.8 broadcast_remainder_fusion
  0.8 0.7 sign_compare_fusion
  1.5 0.1 copy.48
  1.6 0.1 div.36
  1.7 0.1 copy.47
  1.8 0.1 rem.39
  1.9 0.1 copy.46
  2.0 0.1 ne.74
  2.1 0.2 convert_reduce_fusion
  2.3 0.0 copy-start.3
  2.3 0.7 select_reduce_fusion
  3.0 0.7 all_to_all.23
  3.7 8.3 %all-to-all-start = ((s32[16,1,6]{2,1,0:T(1,128)}), s32[16,1,6]{2,1,0:T(1,128)S(1)}, u32[]{:S(2)}, u32[]{:S(2)}) async-start(s32[16,1,6]{2,1,0:T(1,128)} %bitcast), calls=%async_computation | async-start | bytes 16384 | tf_op jit(solution)/shard_map/all_to_all | solution.py:188
  12.0 9.2 %query.1 = (bf16[768,2048]{1,0:T(8,128)(2,1)}, bf16[96,64,256]{2,1,0:T(8,128)(2,1)}) custom-call(s32[96]{0:T(128)} %get-tuple-element.25.slot_span, bf16[768,2048]{1,0:T(8,128)(2,1)} %tok_ref.1, f32[1,2048]{1,0:T(1,128)} %bitcast.31, bf16[2048,256]{1,0:T(8,128)(2,1)} %wq_ref.1), custom_call_target="tpu_custom_call" | custom-call | flops 805306368 | bytes 6291456 | tf_op jit(solution)/shard_map/query/pallas_call | solution.py:193
  21.3 0.0 all-to-all-done
  21.3 0.0 copy-done.3
  21.3 7.0 %all-to-all-start.1 = ((bf16[16,6,64,256]{3,2,1,0:T(8,128)(2,1)}), bf16[16,6,64,256]{3,2,1,0:T(8,128)(2,1)}, u32[]{:S(2)}, u32[]{:S(2)}) async-start(bf16[16,6,64,256]{3,2,1,0:T(8,128)(2,1)} %bitcast.27), calls=%async_computation.1 | async-start | bytes 6291456 | tf_op jit(solution)/shard_map/all_to_all | solution.py:218
  28.2 0.0 copy-start.4
  28.3 0.0 copy-start.1
  28.3 0.0 copy-start.2
  28.3 4.9 %fusion.26 = (f32[768]{0:T(1024)S(1)}, f32[768]{0:T(1024)S(1)}, f32[768,256]{1,0:T(8,128)S(1)}) fusion(bf16[768,2048]{1,0:T(8,128)(2,1)} %get-tuple-element.16, bf16[2048,256]{1,0:T(8,128)(2,1)} %param.21), kind=kOutput, calls=%fused_computation.66 | convolution fusion | flops 818477568 | bytes 4986880 | tf_op jit(solution)/shard_map/dot_general | solution.py:249
  33.1 2.5 %all-reduce = (f32[768]{0:T(1024)S(1)}, f32[768]{0:T(1024)S(1)}) all-reduce(f32[768]{0:T(1024)S(1)} %get-tuple-element.24, f32[768]{0:T(1024)S(1)} %get-tuple-element.23), channel_id=1, replica_groups=mesh['st'=16,'tp'=2] {'tp'}, use_global_device_ids=true, to_apply=%region_6.7 | all-reduce | flops 1536 | bytes 12288 | tf_op jit(solution)/shard_map/psum | solution.py:251
  35.7 0.0 copy-done.4
  35.7 0.3 multiply_convert_fusion
  35.9 0.3 reshape.124
  36.3 0.0 copy-done.1
  36.3 0.0 copy-done.2
  36.3 1.3 fusion.1
  37.6 2.4 %copy.62 = f32[6,128,4,64]{3,2,1,0:T(4,128)} copy(f32[6,128,4,64]{1,3,0,2:T(8,128)} %fusion.1) | data formatting | bytes 1572864 | tf_op jit(solution)/shard_map/reshape | solution.py:262
  40.0 2.2 %reshape.125 = f32[768,256]{1,0:T(8,128)S(1)} reshape(f32[6,128,4,64]{3,2,1,0:T(4,128)} %copy.62) | data formatting | bytes 1572864 | tf_op jit(solution)/shard_map/reshape | solution.py:262
  42.2 4.1 %fusion.3.blend_ref = f32[768,256]{1,0:T(8,128)} fusion(bf16[768,2048]{1,0:T(8,128)(2,1)} %get-tuple-element.16, bf16[2048,256]{1,0:T(8,128)(2,1)} %param.28), kind=kOutput, calls=%fused_computation.6 | convolution fusion | flops 805896192 | bytes 4980736 | tf_op jit(solution)/shard_map/dot_general | solution.py:263
  46.3 15.8 %store.1 = (bf16[24,128,256]{2,1,0:T(8,128)(2,1)}, bf16[24,256,128]{2,1,0:T(8,128)(2,1)}) custom-call(bf16[24,128,2048]{2,1,0:T(8,128)(2,1)} %st_ref.1, f32[1,2048]{1,0:T(1,128)} %bitcast.33, bf16[2048,256]{1,0:T(8,128)(2,1)} %wk_ref.1, bf16[2048,256]{1,0:T(8,128)(2,1)} %wv_ref.1), custom_call_target="tpu_custom_call" | custom-call | flops 6442450944 | bytes 12582912 | tf_op jit(solution)/shard_map/store/pallas_call | solution.py:223
  62.1 5.6 %fusion.6.gated_ref = f32[768,256]{1,0:T(8,128)} fusion(f32[768,256]{1,0:T(8,128)S(1)} %reshape.125, bf16[768,2048]{1,0:T(8,128)(2,1)} %get-tuple-element.16, bf16[2048,256]{1,0:T(8,128)(2,1)} %param.20), kind=kOutput, calls=%fused_computation.11 | convolution fusion | flops 818085888 | bytes 5767168 | tf_op jit(solution)/shard_map/dot_general | solution.py:248
  67.7 0.5 broadcast.309
  68.2 0.6 reduce.3
  68.8 0.6 reshape.115.ids
  69.4 19.6 %all-to-all-done.1.q_ref = bf16[16,6,64,256]{3,2,1,0:T(8,128)(2,1)} async-done(((bf16[16,6,64,256]{3,2,1,0:T(8,128)(2,1)}), bf16[16,6,64,256]{3,2,1,0:T(8,128)(2,1)}, u32[]{:S(2)}, u32[]{:S(2)}) %all-to-all-start.1) | async-done | bytes 3145760 | tf_op jit(solution)/shard_map/all_to_all | solution.py:218
  89.0 92.3 %attention.1 = (bf16[16,6,64,256]{3,2,1,0:T(8,128)(2,1)}, f32[16,6,256]{2,1,0:T(8,128)}) custom-call(s32[96]{0:T(128)} %reshape.115.ids, bf16[16,6,64,256]{3,2,1,0:T(8,128)(2,1)} %all-to-all-done.1.q_ref, bf16[24,128,256]{2,1,0:T(8,128)(2,1)} %get-tuple-element.17.k_ref, bf16[24,256,128]{2,1,0:T(8,128)(2,1)} %get-tuple-element.18.vt_ref), custom_call_target="tpu_custom_call" | custom-call | tf_op jit(solution)/shard_map/attention/pallas_call | solution.py:269
  181.2 1.6 reshape.126.lev_ref
  182.9 5.1 %merge.1 = bf16[768,256]{1,0:T(8,128)(2,1)} custom-call(s32[48]{0:T(128)} %copy-done.3, bf16[96,64,256]{2,1,0:T(8,128)(2,1)} %bitcast.28, f32[96,1,256]{2,1,0:T(1,128)} %reshape.126.lev_ref, f32[768,256]{1,0:T(8,128)} %fusion.6.gated_ref, f32[768,256]{1,0:T(8,128)} %fusion.3.blend_ref), custom_call_target="tpu_custom_call" | custom-call | tf_op jit(solution)/shard_map/merge/pallas_call | solution.py:285
  188.0 1.2 copy.57
  189.2 4.0 %all_to_all.33 = bf16[2,384,256]{1,2,0:T(8,128)(2,1)S(1)} all-to-all(bf16[2,384,256]{1,2,0:T(8,128)(2,1)S(1)} %copy.57), channel_id=1, replica_groups=mesh['st'=16,'tp'=2] {'tp'}, dimensions={0} | all-to-all | bytes 786432 | tf_op jit(solution)/shard_map/all_to_all | solution.py:307
  193.3 0.0 copy-done
  193.3 2.2 %convolution_convert_fusion = bf16[384,2048]{1,0:T(8,128)(2,1)} fusion(bf16[384,512]{0,1:T(8,128)(2,1)S(1)} %bitcast.30, bf16[512,2048]{1,0:T(8,128)(2,1)S(1)} %copy-done), kind=kOutput, calls=%fused_computation | convolution fusion | flops 806092800 | bytes 4063232 | tf_op jit(solution)/shard_map/dot_general | solution.py:308
  (3 shorter events, 0.0 us)
Async XLA Ops:
  0.0 193.3 %copy-start = (bf16[512,2048]{1,0:T(8,128)(2,1)S(1)}, bf16[512,2048]{1,0:T(8,128)(2,1)}, u32[]{:S(2)}) copy-start(bf16[512,2048]{1,0:T(8,128)(2,1)} %param.29) | copy-start | bytes 6291460
  2.3 19.0 %copy-start.3 = (s32[48]{0:T(128)}, s32[48]{0:T(128)S(1)}, u32[]{:S(2)}) copy-start(s32[48]{0:T(128)S(1)} %multiply_add_fusion.pos) | copy-start | bytes 580
  3.7 17.6 %all-to-all-start = ((s32[16,1,6]{2,1,0:T(1,128)}), s32[16,1,6]{2,1,0:T(1,128)S(1)}, u32[]{:S(2)}, u32[]{:S(2)}) async-start(s32[16,1,6]{2,1,0:T(1,128)} %bitcast), calls=%async_computation | async-start | bytes 16384 | tf_op jit(solution)/shard_map/all_to_all | solution.py:188
  21.3 67.7 %all-to-all-start.1 = ((bf16[16,6,64,256]{3,2,1,0:T(8,128)(2,1)}), bf16[16,6,64,256]{3,2,1,0:T(8,128)(2,1)}, u32[]{:S(2)}, u32[]{:S(2)}) async-start(bf16[16,6,64,256]{3,2,1,0:T(8,128)(2,1)} %bitcast.27), calls=%async_computation.1 | async-start | bytes 6291456 | tf_op jit(solution)/shard_map/all_to_all | solution.py:218
  28.2 7.4 %copy-start.4 = (f32[256]{0:T(256)S(1)}, f32[256]{0:T(256)}, u32[]{:S(2)}) copy-start(f32[256]{0:T(256)} %param.22) | copy-start | bytes 3076
  28.3 8.0 %copy-start.1 = (bf16[4,128,128]{2,1,0:T(8,128)(2,1)S(1)}, bf16[4,128,128]{2,1,0:T(8,128)(2,1)}, u32[]{:S(2)}) copy-start(bf16[4,128,128]{2,1,0:T(8,128)(2,1)} %param.23) | copy-start | bytes 393220
  28.3 8.0 %copy-start.2 = (f32[4,128]{1,0:T(4,128)S(1)}, f32[4,128]{1,0:T(4,128)}, u32[]{:S(2)}) copy-start(f32[4,128]{1,0:T(4,128)} %param.24) | copy-start | bytes 6148

commit v2 on v1

--- a/solution.py
+++ b/solution.py
@@ -18,23 +18,10 @@
     return (scaled * gain).astype(bf16)
 
 
-def query_kernel(span_length, slots, slot_span, tok_ref, gain_ref, wq_ref, normed_ref, sent_ref, q_ref):
-    step = pl.program_id(0)
-    rows = tok_ref.shape[0]
+def query_kernel(tok_ref, gain_ref, wq_ref, normed_ref, q_ref):
     normed = normed_rows(tok_ref[...], gain_ref[...])
     normed_ref[...] = normed
-    q = jnp.dot(normed, wq_ref[...], preferred_element_type=f32).astype(bf16)
-    per = rows // span_length
-    for s in range(per):
-        q_ref[step * per + s] = q[s * span_length : (s + 1) * span_length]
-
-    @pl.when(step == pl.num_programs(0) - 1)
-    def _():
-        def body(i, carry):
-            sent_ref[i] = q_ref[slot_span[i]]
-            return carry
-
-        lax.fori_loop(0, slots, body, 0)
+    q_ref[...] = jnp.dot(normed, wq_ref[...], preferred_element_type=f32).astype(bf16)
 
 
 def store_kernel(st_ref, gain_ref, wk_ref, wv_ref, k_ref, vt_ref):
@@ -64,9 +51,8 @@
     return (out / total).astype(bf16), peak + jnp.log(total)
 
 
-def attention_kernel(heads, n, ids, q_ref, k_ref, vt_ref, val_ref, lev_ref, out_val, out_lev, send, recv):
+def attention_kernel(heads, n, cap, ids, picked, q_ref, k_ref, vt_ref, val_ref, lev_ref, out_val, out_lev, send, recv):
     me = lax.axis_index("st")
-    cap = q_ref.shape[1]
 
     barrier = pltpu.get_barrier_semaphore()
 
@@ -85,7 +71,7 @@
     def compute(dst, val_to, lev_to):
         for c in range(cap):
             i = ids[dst * cap + c]
-            val, lev = attend(q_ref[dst, c], k_ref[i], vt_ref[i], heads)
+            val, lev = attend(q_ref[dst, picked[dst * cap + c]], k_ref[i], vt_ref[i], heads)
             val_to[dst, c] = val
             lev_to[dst, c : c + 1] = lev
 
@@ -182,41 +168,40 @@
     order = jnp.arange(requests, dtype=jnp.int32)
     earlier = (owner[:, None] == owner[None, :]) & (order[None, :] < order[:, None])
     position = owner * cap + jnp.sum(earlier.astype(jnp.int32), axis=1)
-    hit = position[None, :] == jnp.arange(slots, dtype=jnp.int32)[:, None]
-    slot_local = jnp.sum(jnp.where(hit, (flat_ids % store_count)[None, :], 0), axis=1)
-    slot_span = jnp.sum(jnp.where(hit, (order // pick_count)[None, :], 0), axis=1)
-    piece_local = lax.all_to_all(
-        slot_local.reshape(owner_count, cap), "st", split_axis=0, concat_axis=0, tiled=True
-    ).reshape(slots)
+
+    asked = lax.all_gather(flat_ids, "st", axis=0, tiled=False)
+    mine = asked // store_count == lax.axis_index("st")
+    before = jnp.sum(
+        jnp.where(mine[:, None, :] & (order[None, None, :] < order[None, :, None]), 1, 0), axis=2
+    )
+    hit = mine[:, None, :] & (before[:, None, :] == jnp.arange(cap, dtype=jnp.int32)[None, :, None])
+    slot_local = jnp.sum(jnp.where(hit, (asked % store_count)[:, None, :], 0), axis=2).reshape(slots)
+    slot_span = jnp.sum(jnp.where(hit, order // pick_count, 0), axis=2).reshape(slots)
 
     tile = 2 * span_length
-    normed, sent = pl.pallas_call(
-        functools.partial(query_kernel, span_length, slots),
-        grid_spec=pltpu.PrefetchScalarGridSpec(
-            num_scalar_prefetch=1,
-            grid=(row_count // tile,),
-            in_specs=[
-                pl.BlockSpec((tile, model), lambda i, _: (i, 0)),
-                pl.BlockSpec((1, model), lambda i, _: (0, 0)),
-                pl.BlockSpec((model, width), lambda i, _: (0, 0)),
-            ],
-            out_specs=[
-                pl.BlockSpec((tile, model), lambda i, _: (i, 0)),
-                pl.BlockSpec((slots, span_length, width), lambda i, _: (0, 0, 0)),
-            ],
-            scratch_shapes=[pltpu.VMEM((span_count, span_length, width), bf16)],
-        ),
+    normed, queries = pl.pallas_call(
+        query_kernel,
+        grid=(row_count // tile,),
+        in_specs=[
+            pl.BlockSpec((tile, model), lambda i: (i, 0)),
+            pl.BlockSpec((1, model), lambda i: (0, 0)),
+            pl.BlockSpec((model, width), lambda i: (0, 0)),
+        ],
+        out_specs=[
+            pl.BlockSpec((tile, model), lambda i: (i, 0)),
+            pl.BlockSpec((tile, width), lambda i: (i, 0)),
+        ],
         out_shape=[
             jax.ShapeDtypeStruct((row_count, model), bf16),
-            jax.ShapeDtypeStruct((slots, span_length, width), bf16),
+            jax.ShapeDtypeStruct((row_count, width), bf16),
         ],
         cost_estimate=pl.CostEstimate(
             flops=2 * row_count * model * width, bytes_accessed=4 * row_count * model, transcendentals=0
         ),
         name="query",
-    )(slot_span, tokens, token_gain.reshape(1, model), query_weight)
-    piece_q = lax.all_to_all(
-        sent.reshape(owner_count, cap, span_length, width), "st", split_axis=0, concat_axis=0, tiled=True
+    )(tokens, token_gain.reshape(1, model), query_weight)
+    all_queries = lax.all_gather(
+        queries.reshape(span_count, span_length, width), "st", axis=0, tiled=False
     )
 
     group = 2
@@ -267,8 +252,8 @@
     level_shape = (owner_count, cap, local_heads * span_length)
     vmem = pl.BlockSpec(memory_space=pltpu.VMEM)
     back_values, back_levels = pl.pallas_call(
-        functools.partial(attention_kernel, local_heads, owner_count),
-        in_specs=[pl.BlockSpec(memory_space=pltpu.SMEM), vmem, vmem, vmem],
+        functools.partial(attention_kernel, local_heads, owner_count, cap),
+        in_specs=[pl.BlockSpec(memory_space=pltpu.SMEM)] * 2 + [vmem] * 3,
         out_specs=[vmem, vmem],
         out_shape=[jax.ShapeDtypeStruct(value_shape, bf16), jax.ShapeDtypeStruct(level_shape, f32)],
         scratch_shapes=[
@@ -279,7 +264,7 @@
         ],
         compiler_params=pltpu.CompilerParams(collective_id=0, has_side_effects=True),
         name="attention",
-    )(piece_local, piece_q, keys, values_t)
+    )(slot_local, slot_span, all_queries, keys, values_t)
 
     spans = 4 if span_count % 4 == 0 else 1
     mixed_rows = pl.pallas_call(

time: 196 us -> 215 us (1.097)
  blocking collectives: 6.55 us -> 50.3 us
  starting transfers between devices: 15.3 us -> 0.01 us
  between operations: 0.16 us -> 13.5 us
  Pallas kernels: 122 us -> 111 us
  waiting for transfers between devices: 19.6 us -> 8.84 us
    all_gather x0 -> x1, blocking collectives: none -> 43.6 us  [per_device(): asked = lax.all_gather(flat_ids, 'st', axis=0, tiled=False)]
    all_to_all x2 -> x0, waiting for transfers between devices: 19.6 us -> none  [the longest x1 19.6 us: per_device(): lax.all_to_all(sent.reshape(owner_count, cap, span_length, width), 'st',...]
    all_to_all x2 -> x0, starting transfers between devices: 15.3 us -> none  [the longest x1 8.34 us: per_device(): lax.all_to_all(slot_local.reshape(owner_count, cap), 'st', split_axis=0,...]
    all_gather x0 -> x1, waiting for transfers between devices: none -> 8.83 us  [per_device(): lax.all_gather(queries.reshape(span_count, span_length, width), 'st', axi...]
    pallas_call x1, Pallas kernels: 92.3 us -> 83.7 us  [per_device(): pl.pallas_call(functools.partial(attention_kernel, local_heads, owner_cou...]
    pallas_call x1, Pallas kernels: 9.21 us -> 6.45 us  [per_device(): pl.pallas_call(query_kernel, grid=(row_count // tile,), in_specs=[pl.Bloc...]
  transfers between devices with their start and end apart: 2 -> 1, of which waited for: 1 -> 1; matrix products, arithmetic and copies ran while one was open for 12% -> 12% of each run, Pallas kernels for 13% -> 7%
where the time goes in v2:
time: 215 us; the launch traced here: 214 us
  Pallas kernels  111 us (52%)
  blocking collectives  50.3 us (23%)
  matrix products  18 us (8%)
  between operations  13.5 us (6%)
  local copies, waits for them, and re-layouts  9.93 us (5%)
  waiting for transfers between devices  8.84 us (4%)
  other arithmetic  2.4 us (1%)
    pallas_call x1, Pallas kernels, per_device(): pl.pallas_call(functools.partial(attention_kernel, local_heads, owner_cou...  83.7 us
    all_gather x1, blocking collectives, per_device(): asked = lax.all_gather(flat_ids, 'st', axis=0, tiled=False)  43.6 us
    pallas_call x1, Pallas kernels, per_device(): pl.pallas_call(store_kernel, grid=(store_count // group,), in_specs=[pl.B...  15.8 us
    all_gather x1, waiting for transfers between devices, per_device(): lax.all_gather(queries.reshape(span_count, span_length, width), 'st', axi...  8.83 us
    pallas_call x1, Pallas kernels, per_device(): pl.pallas_call(query_kernel, grid=(row_count // tile,), in_specs=[pl.Bloc...  6.45 us
    dot_general x1, matrix products, per_device(): carry_branch = jnp.dot(normed, carry_weight, preferred_element_type=f32)  5.58 us
    pallas_call x1, Pallas kernels, per_device(): pl.pallas_call(functools.partial(merge_kernel, local_heads, spans, pick_c...  5.14 us
    dot_general x1, matrix products, per_device(): jnp.dot(normed, spatial_weight, preferred_element_type=f32)  4.87 us
  transfers between devices with their start and end apart: 1, of which 1 were waited for; matrix products, arithmetic and copies ran while one was open for 12% of the time, Pallas kernels for 7%

profile of v2, /device:TPU:0, one launch (start us, length us, event | category | flops | bytes accessed | tf_op | source)
XLA Modules:
  0.0 214.2 jit_solution(1159501388004440244)
XLA Ops:
  6.5 0.0 copy-start
  6.5 0.0 all-gather.3.cloned.1.call-start
  6.5 6.4 %query.1 = (bf16[768,2048]{1,0:T(8,128)(2,1)}, bf16[768,256]{1,0:T(8,128)(2,1)}) custom-call(bf16[768,2048]{1,0:T(8,128)(2,1)} %tok_ref.1, f32[1,2048]{1,0:T(1,128)} %bitcast.46, bf16[2048,256]{1,0:T(8,128)(2,1)} %wq_ref.1), custom_call_target="tpu_custom_call" | custom-call | flops 805306368 | bytes 6291456 | tf_op jit(solution)/shard_map/query/pallas_call | solution.py:182
  13.0 0.0 all-gather.3.cloned.1.call-update
  13.0 0.0 copy-start.4
  13.0 0.0 copy-start.1
  13.0 0.0 copy-start.3
  13.1 4.9 %fusion.30 = (f32[768]{0:T(1024)S(1)}, f32[768]{0:T(1024)S(1)}, f32[768,256]{1,0:T(8,128)S(1)}) fusion(bf16[768,2048]{1,0:T(8,128)(2,1)} %get-tuple-element.16, bf16[2048,256]{1,0:T(8,128)(2,1)} %param.21), kind=kOutput, calls=%fused_computation.74 | convolution fusion | flops 818477568 | bytes 4986880 | tf_op jit(solution)/shard_map/dot_general | solution.py:234
  17.9 2.7 %all-reduce = (f32[768]{0:T(1024)S(1)}, f32[768]{0:T(1024)S(1)}) all-reduce(f32[768]{0:T(1024)S(1)} %get-tuple-element.24, f32[768]{0:T(1024)S(1)} %get-tuple-element.23), channel_id=1, replica_groups=mesh['st'=16,'tp'=2] {'tp'}, use_global_device_ids=true, to_apply=%region_7.8 | all-reduce | flops 1536 | bytes 12288 | tf_op jit(solution)/shard_map/psum | solution.py:236
  20.6 0.0 copy-done.4
  20.6 0.3 multiply_convert_fusion
  20.9 0.3 reshape.122
  21.2 0.0 copy-done.1
  21.2 0.0 copy-done.3
  21.2 1.3 fusion.1
  22.5 2.5 %copy.74 = f32[6,128,4,64]{3,2,1,0:T(4,128)} copy(f32[6,128,4,64]{1,3,0,2:T(8,128)} %fusion.1) | data formatting | bytes 1572864 | tf_op jit(solution)/shard_map/reshape | solution.py:247
  25.0 2.3 %reshape.123 = f32[768,256]{1,0:T(8,128)S(1)} reshape(f32[6,128,4,64]{3,2,1,0:T(4,128)} %copy.74) | data formatting | bytes 1572864 | tf_op jit(solution)/shard_map/reshape | solution.py:247
  27.3 4.1 %fusion.3.blend_ref = f32[768,256]{1,0:T(8,128)} fusion(bf16[768,2048]{1,0:T(8,128)(2,1)} %get-tuple-element.16, bf16[2048,256]{1,0:T(8,128)(2,1)} %param.28), kind=kOutput, calls=%fused_computation.6 | convolution fusion | flops 805896192 | bytes 4980736 | tf_op jit(solution)/shard_map/dot_general | solution.py:248
  31.4 15.8 %store.1 = (bf16[24,128,256]{2,1,0:T(8,128)(2,1)}, bf16[24,256,128]{2,1,0:T(8,128)(2,1)}) custom-call(bf16[24,128,2048]{2,1,0:T(8,128)(2,1)} %st_ref.1, f32[1,2048]{1,0:T(1,128)} %bitcast.48, bf16[2048,256]{1,0:T(8,128)(2,1)} %wk_ref.1, bf16[2048,256]{1,0:T(8,128)(2,1)} %wv_ref.1), custom_call_target="tpu_custom_call" | custom-call | flops 6442450944 | bytes 12582912 | tf_op jit(solution)/shard_map/store/pallas_call | solution.py:208
  47.2 0.0 copy-start.2
  47.2 5.6 %fusion.6.gated_ref = f32[768,256]{1,0:T(8,128)} fusion(f32[768,256]{1,0:T(8,128)S(1)} %reshape.123, bf16[768,2048]{1,0:T(8,128)(2,1)} %get-tuple-element.16, bf16[2048,256]{1,0:T(8,128)(2,1)} %param.20), kind=kOutput, calls=%fused_computation.11 | convolution fusion | flops 818085888 | bytes 5767168 | tf_op jit(solution)/shard_map/dot_general | solution.py:233
  52.8 0.0 copy-done.2
  52.8 0.1 copy.56
  52.9 0.1 reshape.111
  53.0 43.6 %all-gather = s32[16,1,48]{2,1,0:T(1,128)S(1)} all-gather(s32[1,1,48]{2,1,0:T(1,128)S(1)} %reshape.111), channel_id=1, replica_groups=mesh['st'=16,'tp'=2] {'st'}, dimensions={0}, use_global_device_ids=true | all-gather | bytes 3264 | tf_op jit(solution)/shard_map/all_gather | solution.py:172
  96.6 0.7 rem.41
  97.3 0.4 select_reduce_fusion
  97.7 0.3 select_reduce_fusion.1
  98.0 0.1 copy.60
  98.0 0.6 reshape.103.ids
  98.7 0.1 copy.61
  98.8 0.6 reshape.104.picked
  99.4 0.1 copy.55
  99.5 0.1 div.39
  99.6 0.1 copy.54
  99.7 0.1 and.53
  99.8 0.2 convert_reduce_fusion
  100.0 0.6 multiply_add_fusion.pos
  100.6 8.8 %all-gather.3.cloned.1.call-done.q_ref = bf16[16,12,64,256]{3,2,1,0:T(8,128)(2,1)} async-done(((bf16[1,12,64,256]{3,2,1,0:T(8,128)(2,1)}), bf16[16,12,64,256]{3,2,1,0:T(8,128)(2,1)}) %all-gather.3.cloned.1.call-update) | async-done | bytes 6291472 | tf_op jit(solution)/shard_map/all_gather | solution.py:203
  109.4 83.7 %attention.1 = (bf16[16,6,64,256]{3,2,1,0:T(8,128)(2,1)}, f32[16,6,256]{2,1,0:T(8,128)}) custom-call(s32[96]{0:T(128)} %reshape.103.ids, s32[96]{0:T(128)} %reshape.104.picked, bf16[16,12,64,256]{3,2,1,0:T(8,128)(2,1)} %all-gather.3.cloned.1.call-done.q_ref, bf16[24,128,256]{2,1,0:T(8,128)(2,1)} %get-tuple-element.17.k_ref, ...), custom_call_target="tpu_custom_call" | custom-call | tf_op jit(solution)/shard_map/attention/pallas_call | solution.py:254
  193.1 1.6 reshape.124.lev_ref
  194.8 5.1 %merge.1 = bf16[768,256]{1,0:T(8,128)(2,1)} custom-call(s32[48]{0:T(128)} %multiply_add_fusion.pos, bf16[96,64,256]{2,1,0:T(8,128)(2,1)} %bitcast.38, f32[96,1,256]{2,1,0:T(1,128)} %reshape.124.lev_ref, f32[768,256]{1,0:T(8,128)} %fusion.6.gated_ref, f32[768,256]{1,0:T(8,128)} %fusion.3.blend_ref), custom_call_target="tpu_custom_call" | custom-call | tf_op jit(solution)/shard_map/merge/pallas_call | solution.py:270
  199.9 1.2 copy.69
  201.1 4.0 %all_to_all.19 = bf16[2,384,256]{1,2,0:T(8,128)(2,1)S(1)} all-to-all(bf16[2,384,256]{1,2,0:T(8,128)(2,1)S(1)} %copy.69), channel_id=1, replica_groups=mesh['st'=16,'tp'=2] {'tp'}, dimensions={0} | all-to-all | bytes 786432 | tf_op jit(solution)/shard_map/all_to_all | solution.py:292
  205.2 0.0 copy-done
  205.2 2.2 %convolution_convert_fusion = bf16[384,2048]{1,0:T(8,128)(2,1)} fusion(bf16[384,512]{0,1:T(8,128)(2,1)S(1)} %bitcast.40, bf16[512,2048]{1,0:T(8,128)(2,1)S(1)} %copy-done), kind=kOutput, calls=%fused_computation | convolution fusion | flops 806092800 | bytes 4063232 | tf_op jit(solution)/shard_map/dot_general | solution.py:293
  (9 shorter events, 0.1 us)
Async XLA Ops:
  6.5 198.6 %copy-start = (bf16[512,2048]{1,0:T(8,128)(2,1)S(1)}, bf16[512,2048]{1,0:T(8,128)(2,1)}, u32[]{:S(2)}) copy-start(bf16[512,2048]{1,0:T(8,128)(2,1)} %param.29) | copy-start | bytes 6291460
  6.5 102.8 %all-gather.3.cloned.1.call-start = ((), (), s32[]{:S(2)}) async-start(), calls=%async_computation.1 | async-start | bytes 6684672 | tf_op jit(solution)/shard_map/all_gather | solution.py:203
  13.0 7.6 %copy-start.4 = (f32[256]{0:T(256)S(1)}, f32[256]{0:T(256)}, u32[]{:S(2)}) copy-start(f32[256]{0:T(256)} %param.22) | copy-start | bytes 3076
  13.0 8.2 %copy-start.1 = (bf16[4,128,128]{2,1,0:T(8,128)(2,1)S(1)}, bf16[4,128,128]{2,1,0:T(8,128)(2,1)}, u32[]{:S(2)}) copy-start(bf16[4,128,128]{2,1,0:T(8,128)(2,1)} %param.23) | copy-start | bytes 393220
  13.0 8.2 %copy-start.3 = (f32[4,128]{1,0:T(4,128)S(1)}, f32[4,128]{1,0:T(4,128)}, u32[]{:S(2)}) copy-start(f32[4,128]{1,0:T(4,128)} %param.24) | copy-start | bytes 6148
  47.2 5.6 %copy-start.2 = (s32[12,4]{0,1:T(4,128)S(1)}, s32[12,4]{0,1:T(4,128)}, u32[]{:S(2)}) copy-start(s32[12,4]{0,1:T(4,128)} %param.16) | copy-start | bytes 580
Sparse Core Ops, SparseCore 0:
  13.1 96.2 all-gather.2
